TPU v7x, 32 devices: a whole 2x2x4 slice. The times are simulated.
32 devices in a mesh: grp: 2 (over y), sp: 4 (over z), fs: 2 (over x), tp: 2 (over core).
Axes of the slice: x: 2, y: 2, z: 4, core: 2. Of those that a mesh axis runs over, the one named last changes fastest.
Arguments:
- tokens: bfloat16 [4, 512, 2048], P(('grp', 'fs'), 'sp', 'tp'), parts along dimension 0, may hold values from -120 to 120
- mix_gain: float32 [2048], replicated, may hold values from 0.1 to 1.9
- attn_query: bfloat16 [2048, 1024], P('fs', 'tp'), may hold values from -0.375 to 0.375
- attn_key: bfloat16 [2048, 1024], P('fs', 'tp'), may hold values from -0.125 to 0.125
- attn_value: bfloat16 [2048, 1024], P('fs', 'tp'), may hold values from -0.125 to 0.125
- rec_query: bfloat16 [2048, 1024], P('fs', 'tp'), may hold values from -0.125 to 0.125
- rec_forget: bfloat16 [2048, 1024], P('fs', 'tp'), may hold values from -0.125 to 0.125
- rec_input: bfloat16 [2048, 1024], P('fs', 'tp'), may hold values from -0.125 to 0.125
- break_offset: float32 [8], P('tp'), may hold values from -13.5 to -7
- forget_room: float32 [8, 128], P('tp'), may hold values from 0.0009765625 to 0.05
- out_gain: float32 [128], replicated, may hold values from 0.1 to 1.9
- out_attn: bfloat16 [1024, 2048], P('tp', 'fs'), may hold values from -0.125 to 0.125
- out_rec: bfloat16 [1024, 2048], P('tp', 'fs'), may hold values from -0.125 to 0.125
Outputs:
- mixed: bfloat16 [4, 512, 2048], P(('grp', 'fs'), ('sp', 'tp')), parts along dimension 0
There are 2 independent parts, one for each index of `grp`. A program takes and returns all parts, laid end to end along the dimension named above; an argument that names none is the same for every part. Nothing has to cross between parts.
All inputs are finite; a program needn't handle non-finite values.
Results may differ from a plain program's by a relative error of at most 0.019.
Values may be sent and summed in bfloat16 or wider, within the bound.
A program may use at most 64 MiB of HBM per device.

v0:
```python
import math
import jax
import jax.numpy as jnp
from jax import lax
from jax.sharding import PartitionSpec as P

HEAD = 128
DK = 128
DV = 128
REC_BLOCK = 64
norm_eps = 1e-06
highest = lax.Precision.HIGHEST


def carried_in(x, axis, join, neutral):
    place = lax.axis_index(axis)
    gathered = jax.tree.map(
        lambda a, kind: lax.all_gather(a.astype(kind), axis), x, (jnp.bfloat16, jnp.bfloat16)
    )
    state = jax.tree.map(lambda a, e: jnp.zeros_like(a) + jnp.asarray(e, a.dtype), x, neutral)

    def one(step, state):
        return join(
            state,
            jax.tree.map(
                lambda a, own: lax.dynamic_index_in_dim(a, step, 0, False).astype(own.dtype),
                gathered,
                x,
            ),
        )

    return lax.fori_loop(0, place, one, state)


def block_step(states, inputs):
    queries, key_in, value_rows, log_forget = inputs
    block_len = queries.shape[-2]
    cum_log = jnp.cumsum(log_forget, axis=-2)
    last_log = cum_log[..., -1:, :]
    q_dec = queries * jnp.exp(cum_log)
    k_inv = key_in * jnp.exp(-cum_log)
    causal = lax.iota(jnp.int32, block_len)[:, None] >= lax.iota(jnp.int32, block_len)[None, :]
    carried_part = jnp.einsum("...tk,...kv->...tv", q_dec, states, precision=highest)
    scores = jnp.where(
        causal, jnp.einsum("...tk,...sk->...ts", q_dec, k_inv, precision=highest), 0.0
    )
    inner_part = jnp.einsum("...ts,...sv->...tv", scores, value_rows, precision=highest)
    fresh_state = jnp.einsum(
        "...sk,...sv->...kv", key_in * jnp.exp(last_log - cum_log), value_rows, precision=highest
    )
    return (
        jnp.exp(jnp.swapaxes(last_log, -1, -2)) * states + fresh_state,
        carried_part + inner_part,
    )


def stick_mixer(queries, key_rows, value_rows, offsets):
    seq_count, tok_rows, head_count, head_width = queries.shape
    own_index = lax.axis_index("sp")
    sp_count = lax.axis_size("sp")
    factor = 1.0 / math.sqrt(head_width)
    q_pos = own_index * tok_rows + lax.iota(jnp.int32, tok_rows)
    start_acc = jnp.zeros((sp_count, seq_count, tok_rows, head_count, head_width), jnp.float32)
    start_log = jnp.zeros((sp_count, seq_count, tok_rows, head_count), jnp.float32)

    def one_block(carried, key_blk, value_blk, slot):

        def compute(states):
            sums_acc, log_sums = states
            scores = jnp.einsum(
                "bqhe,bkhe->bhqk", queries, key_blk, preferred_element_type=jnp.float32
            )
            scores = scores * factor + offsets[None, :, None, None]
            k_pos = slot * tok_rows + lax.iota(jnp.int32, tok_rows)
            strict = k_pos[None, :] < q_pos[:, None]
            log_keep = jnp.where(strict, jax.nn.log_sigmoid(-scores), 0.0)
            inner_sum = lax.cumsum(log_keep, axis=3, reverse=True) - log_keep
            sticks = jnp.where(strict, jnp.exp(jax.nn.log_sigmoid(scores) + inner_sum), 0.0).astype(
                jnp.bfloat16
            )
            partial_value = jnp.einsum(
                "bhqk,bkhe->bqhe", sticks, value_blk, preferred_element_type=jnp.float32
            )
            totals = jnp.transpose(jnp.sum(log_keep, axis=3), (0, 2, 1))
            return (
                lax.dynamic_update_index_in_dim(sums_acc, partial_value, slot, 0),
                lax.dynamic_update_index_in_dim(log_sums, totals, slot, 0),
            )

        return lax.cond(slot <= own_index, compute, lambda states: states, carried)

    key_all = lax.all_gather(key_rows, "sp", axis=1, tiled=True)
    value_all = lax.all_gather(value_rows, "sp", axis=1, tiled=True)
    blocks = key_all.shape[1] // tok_rows

    def turn(block_idx, states):
        key_blk = lax.dynamic_slice_in_dim(key_all, block_idx * tok_rows, tok_rows, 1)
        value_blk = lax.dynamic_slice_in_dim(value_all, block_idx * tok_rows, tok_rows, 1)
        return one_block(states, key_blk, value_blk, block_idx)

    sums_acc, log_sums = lax.fori_loop(0, blocks, turn, (start_acc, start_log))
    later_sum = jnp.cumsum(log_sums[::-1], axis=0)[::-1] - log_sums
    return jnp.sum(sums_acc * jnp.exp(later_sum)[..., None], axis=0).astype(jnp.bfloat16)


def combine_states(earlier, later):
    return (earlier[0] + later[0], jnp.exp(later[0])[..., None] * earlier[1] + later[1])


def recur_mixer(queries, gate_pre, inputs, rooms, gain):
    seq_count, tok_rows, head_count, key_dim = queries.shape
    val_dim = inputs.shape[3]
    key_in = rooms * jax.nn.sigmoid(-gate_pre.astype(jnp.float32))
    log_forget = jnp.log1p(-key_in)
    query32 = queries.astype(jnp.float32)
    blocks = tok_rows // REC_BLOCK

    def split_blocks(tensor):
        return jnp.transpose(
            tensor.reshape(seq_count, blocks, REC_BLOCK, head_count, tensor.shape[3]),
            (1, 0, 3, 2, 4),
        )

    empty_state = jnp.zeros((seq_count, head_count, key_dim, val_dim), jnp.float32)
    final_state, pieces = lax.scan(
        block_step,
        empty_state,
        (
            split_blocks(query32),
            split_blocks(key_in),
            split_blocks(inputs.astype(jnp.float32)),
            split_blocks(log_forget),
        ),
    )
    local_out = jnp.transpose(pieces, (1, 0, 3, 2, 4)).reshape(
        seq_count, tok_rows, head_count, val_dim
    )
    running = jnp.cumsum(log_forget, axis=1)
    identity = (jnp.zeros((seq_count, head_count, key_dim), jnp.float32), empty_state)
    incoming = carried_in((running[:, -1], final_state), "sp", combine_states, identity)[1]
    raw_out = local_out + jnp.einsum(
        "bthk,bhkv->bthv", query32 * jnp.exp(running), incoming, precision=highest
    )
    factor = lax.rsqrt(jnp.mean(raw_out * raw_out, axis=3, keepdims=True) + norm_eps)
    return (raw_out * factor * gain).astype(jnp.bfloat16)


def body(
    tokens,
    mix_gain,
    attn_query,
    attn_key,
    attn_value,
    rec_query,
    rec_forget,
    rec_input,
    break_offset,
    forget_room,
    out_gain,
    out_attn,
    out_rec,
):
    whole = lax.all_gather(tokens, "tp", axis=2, tiled=True)
    seq_rows = whole.shape[1]
    model_width = whole.shape[2]
    rows32 = whole.astype(jnp.float32)
    factor = lax.rsqrt(jnp.mean(rows32 * rows32, axis=2, keepdims=True) + norm_eps)
    normed = (rows32 * factor * mix_gain).astype(jnp.bfloat16).reshape(seq_rows, model_width)
    weights = (attn_query, attn_key, attn_value, rec_query, rec_forget, rec_input)
    turned = (
        lax.all_to_all(weights[0], "fs", split_axis=1, concat_axis=0, tiled=True),
        lax.all_to_all(weights[1], "fs", split_axis=1, concat_axis=0, tiled=True),
        lax.all_to_all(weights[2], "fs", split_axis=1, concat_axis=0, tiled=True),
        lax.all_to_all(weights[3], "fs", split_axis=1, concat_axis=0, tiled=True),
        lax.all_to_all(weights[4], "fs", split_axis=1, concat_axis=0, tiled=True),
        lax.all_to_all(weights[5], "fs", split_axis=1, concat_axis=0, tiled=True),
    )
    pieces = lax.all_gather(normed, "fs", axis=0, tiled=True)
    projected = tuple(
        (
            jnp.dot(pieces, matrix, preferred_element_type=jnp.float32).astype(jnp.bfloat16)
            for matrix in turned
        )
    )
    seq_count = lax.axis_size("fs")
    own_fs = lax.axis_index("fs")
    attn_heads = break_offset.shape[0] // seq_count
    rec_heads = forget_room.shape[0] // seq_count
    offsets = lax.dynamic_slice_in_dim(break_offset, own_fs * attn_heads, attn_heads, 0)
    rooms = lax.dynamic_slice_in_dim(forget_room, own_fs * rec_heads, rec_heads, 0)

    def heads_of(matrix, width_each):
        return matrix.reshape(seq_count, seq_rows, matrix.shape[1] // width_each, width_each)

    attn_out = stick_mixer(
        heads_of(projected[0], HEAD),
        heads_of(projected[1], HEAD),
        heads_of(projected[2], HEAD),
        offsets,
    )
    rec_out = recur_mixer(
        heads_of(projected[3], DK),
        heads_of(projected[4], DK),
        heads_of(projected[5], DV),
        rooms,
        out_gain,
    )
    attn_flat = attn_out.reshape(seq_count * seq_rows, -1)
    rec_flat = rec_out.reshape(seq_count * seq_rows, -1)
    attn_flat, rec_flat = (
        lax.all_to_all(attn_flat, "fs", split_axis=0, concat_axis=1, tiled=True),
        lax.all_to_all(rec_flat, "fs", split_axis=0, concat_axis=1, tiled=True),
    )
    full_attn, full_rec = (
        lax.all_gather(out_attn, "fs", axis=1, tiled=True),
        lax.all_gather(out_rec, "fs", axis=1, tiled=True),
    )
    share = seq_rows // lax.axis_size("tp")
    mixed = lax.psum_scatter(
        (
            jnp.dot(attn_flat, full_attn, preferred_element_type=jnp.float32)
            + jnp.dot(rec_flat, full_rec, preferred_element_type=jnp.float32)
        ).astype(jnp.bfloat16),
        "tp",
        scatter_dimension=0,
        tiled=True,
    )
    return mixed.reshape(1, share, model_width)


def solution(mesh):
    placed = (
        P(("grp", "fs"), "sp", "tp"),
        P(),
        P("fs", "tp"),
        P("fs", "tp"),
        P("fs", "tp"),
        P("fs", "tp"),
        P("fs", "tp"),
        P("fs", "tp"),
        P("tp"),
        P("tp", None),
        P(),
        P("tp", "fs"),
        P("tp", "fs"),
    )
    return jax.shard_map(
        body,
        mesh=mesh,
        in_specs=placed,
        out_specs=P(("grp", "fs"), ("sp", "tp"), None),
        check_vma=False,
    )
```

profile of v0, /device:TPU:0, one launch (start us, length us, event | category | flops | bytes accessed | tf_op | source)
XLA Modules:
  0.0 285.6 jit_solution(8007163119693888808)
XLA Ops:
  6.5 2.6 all_gather.28
  9.4 1.7 fusion.54
  11.1 1.3 copy.92
  12.4 4.1 %all-to-all-start.4 = ((bf16[1024,2,256]{0,2,1:T(8,128)(2,1)}), bf16[1024,2,256]{0,2,1:T(8,128)(2,1)S(1)}, u32[]{:S(2)}, u32[]{:S(2)}) async-start(bf16[1024,2,256]{0,2,1:T(8,128)(2,1)} %bitcast.20), calls=%async_computation.4 | async-start | bytes 2097152 | tf_op jit(solution)/shard_map/all_to_all | solution.py:175
  17.9 21.6 %all-to-all-done.4 = bf16[1024,2,256]{0,2,1:T(8,128)(2,1)S(1)} async-done(((bf16[1024,2,256]{0,2,1:T(8,128)(2,1)}), bf16[1024,2,256]{0,2,1:T(8,128)(2,1)S(1)}, u32[]{:S(2)}, u32[]{:S(2)}) %all-to-all-start.4) | async-done | bytes 1048608 | tf_op jit(solution)/shard_map/all_to_all | solution.py:175
  39.4 3.6 %all-to-all-start.6 = ((bf16[1024,2,256]{0,2,1:T(8,128)(2,1)}), bf16[1024,2,256]{0,2,1:T(8,128)(2,1)S(1)}, u32[]{:S(2)}, u32[]{:S(2)}) async-start(bf16[1024,2,256]{0,2,1:T(8,128)(2,1)} %bitcast.29), calls=%async_computation.6 | async-start | bytes 2097152 | tf_op jit(solution)/shard_map/all_to_all | solution.py:174
  45.1 10.5 %all-to-all-done.6 = bf16[1024,2,256]{0,2,1:T(8,128)(2,1)S(1)} async-done(((bf16[1024,2,256]{0,2,1:T(8,128)(2,1)}), bf16[1024,2,256]{0,2,1:T(8,128)(2,1)S(1)}, u32[]{:S(2)}, u32[]{:S(2)}) %all-to-all-start.6) | async-done | bytes 1048608 | tf_op jit(solution)/shard_map/all_to_all | solution.py:174
  55.6 3.6 %all-to-all-start.5 = ((bf16[1024,2,256]{0,2,1:T(8,128)(2,1)}), bf16[1024,2,256]{0,2,1:T(8,128)(2,1)S(1)}, u32[]{:S(2)}, u32[]{:S(2)}) async-start(bf16[1024,2,256]{0,2,1:T(8,128)(2,1)} %bitcast.144), calls=%async_computation.5 | async-start | bytes 2097152 | tf_op jit(solution)/shard_map/all_to_all | solution.py:176
  59.2 2.3 copy.82
  61.5 22.8 %all-to-all-done.5 = bf16[1024,2,256]{0,2,1:T(8,128)(2,1)S(1)} async-done(((bf16[1024,2,256]{0,2,1:T(8,128)(2,1)}), bf16[1024,2,256]{0,2,1:T(8,128)(2,1)S(1)}, u32[]{:S(2)}, u32[]{:S(2)}) %all-to-all-start.5) | async-done | bytes 1048608 | tf_op jit(solution)/shard_map/all_to_all | solution.py:176
  84.3 4.4 %all-to-all-start = ((bf16[1024,2,256]{0,2,1:T(8,128)(2,1)}), bf16[1024,2,256]{0,2,1:T(8,128)(2,1)}, u32[]{:S(2)}, u32[]{:S(2)}) async-start(bf16[1024,2,256]{0,2,1:T(8,128)(2,1)} %bitcast.145), calls=%async_computation | async-start | bytes 2097152 | tf_op jit(solution)/shard_map/all_to_all | solution.py:172
  88.7 2.3 copy.87
  91.1 12.6 %all-to-all-done = bf16[1024,2,256]{0,2,1:T(8,128)(2,1)} async-done(((bf16[1024,2,256]{0,2,1:T(8,128)(2,1)}), bf16[1024,2,256]{0,2,1:T(8,128)(2,1)}, u32[]{:S(2)}, u32[]{:S(2)}) %all-to-all-start) | async-done | bytes 1048608 | tf_op jit(solution)/shard_map/all_to_all | solution.py:172
  103.7 4.5 %all-to-all-start.2 = ((bf16[1024,2,256]{0,2,1:T(8,128)(2,1)}), bf16[1024,2,256]{0,2,1:T(8,128)(2,1)}, u32[]{:S(2)}, u32[]{:S(2)}) async-start(bf16[1024,2,256]{0,2,1:T(8,128)(2,1)} %bitcast.146), calls=%async_computation.2 | async-start | bytes 2097152 | tf_op jit(solution)/shard_map/all_to_all | solution.py:173
  108.1 2.3 copy.85
  110.4 10.6 %all-to-all-done.2 = bf16[1024,2,256]{0,2,1:T(8,128)(2,1)} async-done(((bf16[1024,2,256]{0,2,1:T(8,128)(2,1)}), bf16[1024,2,256]{0,2,1:T(8,128)(2,1)}, u32[]{:S(2)}, u32[]{:S(2)}) %all-to-all-start.2) | async-done | bytes 1048608 | tf_op jit(solution)/shard_map/all_to_all | solution.py:173
  121.1 4.4 %all-to-all-start.1 = ((bf16[1024,2,256]{0,2,1:T(8,128)(2,1)}), bf16[1024,2,256]{0,2,1:T(8,128)(2,1)}, u32[]{:S(2)}, u32[]{:S(2)}) async-start(bf16[1024,2,256]{0,2,1:T(8,128)(2,1)} %bitcast.141), calls=%async_computation.1 | async-start | bytes 2097152 | tf_op jit(solution)/shard_map/all_to_all | solution.py:171
  126.3 1.3 copy.93
  129.0 1.4 copy.96
  130.3 2.3 copy.83
  132.6 2.4 copy.88
  134.9 2.6 all-to-all-done.1
  137.5 1.5 copy.86
  139.1 2.5 fusion.51
  141.6 1.8 div.26
  143.4 1.9 div.27
  145.3 2.4 fusion.46
  147.7 1.8 reshape.147
  149.4 1.8 reshape.145
  153.4 1.8 fusion.66
  156.2 6.9 %while.43 = (s32[]{:T(128)}, f32[2,2,128,128]{3,2,1,0:T(8,128)S(1)}, f32[2,2,2,64,128]{4,3,0,2,1:T(8,128)}, f32[2,2,2,64,128]{4,3,2,1,0:T(8,128)}, f32[2,2,2,64,...) while((s32[]{:T(128)}, ...), condition=%wide.region_11.12_spmd.clone, body=%wide.region_9.11_spmd.clone.sunk | while | flops 153571328 | bytes 3239036 | solution.py:125
  163.1 16.6 %all-gather.2 = bf16[8,2,128,128]{3,2,1,0:T(8,128)(2,1)} all-gather(bf16[2,2,128,128]{3,2,1,0:T(8,128)(2,1)S(1)} %convert_element_type.118), channel_id=4, replica_groups=mesh['grp'=2,'sp'=4,'fs'=2,'tp'=2] {'sp'}, dimensions={0}, use_global_device_ids=true | all-gather | bytes 655360 | tf_op jit(solution)/shard_map/all_gather | solution.py:18
  179.8 2.3 exponential_multiply_fusion
  182.0 9.4 %all-gather.1 = bf16[8,1,2,128]{3,2,1,0:T(2,128)(2,1)S(1)} all-gather(bf16[2,1,2,128]{3,2,1,0:T(2,128)(2,1)S(1)} %slice.12), channel_id=3, replica_groups=mesh['grp'=2,'sp'=4,'fs'=2,'tp'=2] {'sp'}, dimensions={0}, use_global_device_ids=true | all-gather | bytes 5120 | tf_op jit(solution)/shard_map/all_gather | solution.py:18
  191.5 1.8 copy.104
  193.3 1.7 convolution_convert_fusion.5
  195.0 16.5 %all_gather.30 = bf16[2,512,2,128]{3,1,2,0:T(8,128)(2,1)} all-gather(bf16[2,128,2,128]{3,1,2,0:T(8,128)(2,1)S(1)} %copy.84), channel_id=1, replica_groups=mesh['grp'=2,'sp'=4,'fs'=2,'tp'=2] {'sp'}, dimensions={1}, use_global_device_ids=true | all-gather | bytes 655360 | tf_op jit(solution)/shard_map/all_gather | solution.py:92
  212.1 14.9 %all_gather.31 = bf16[2,512,2,128]{3,1,2,0:T(8,128)(2,1)S(1)} all-gather(bf16[2,128,2,128]{3,1,2,0:T(8,128)(2,1)S(1)} %copy.89), channel_id=1, replica_groups=mesh['grp'=2,'sp'=4,'fs'=2,'tp'=2] {'sp'}, dimensions={1}, use_global_device_ids=true | all-gather | bytes 655360 | tf_op jit(solution)/shard_map/all_gather | solution.py:93
  227.6 6.6 %while.42 = (s32[]{:T(128)}, f32[4,2,128,2,128]{4,2,3,1,0:T(8,128)S(1)}, f32[4,2,128,2]{2,3,1,0:T(2,128)S(1)}, s32[]{:T(128)}, bf16[2,512,2,128]{3,1,2,0:T(8,128...) while((s32[]{:T(128)}, ...), condition=%wide.region_6.7_spmd.clone, body=%wide.region_1.6_spmd.clone.sunk | while | flops 43925260 | bytes 2286935 | solution.py:101
  227.7 6.4 %conditional.3 = ((f32[4,2,128,2,128]{4,2,3,1,0:T(8,128)S(1)}, f32[4,2,128,2]{2,3,1,0:T(2,128)S(1)})) conditional(s32[]{:T(128)} %convert_element_type.168, (f32[4,2,128,2,128]{4,2,3,1,0:T(8,128)S(1)}, f32[4,2,128,2]{2,3,1,0:T(2,128)S(1)}) %tuple.100, (s32[]{:T(128)}, s32[]{:T(128)}, bf16[2,512,2,128]{3,1,2,0:T(8,128)(2,1)}, ...), branch_computations={%region_2.0_spmd, %region_3.5_spmd} | conditional | flops 43925256 | bytes 2286220 | solution.py:90
  229.1 4.4 %reduce_window_sum.43 = f32[2,2,128,128]{2,3,1,0:T(8,128)S(1)} reduce-window(f32[2,2,128,128]{2,3,1,0:T(8,128)S(1)} %get-tuple-element.514, f32[]{:T(128)} %constant.131.clone), window={size=1x1x1x128 pad=0_0x0_0x0_0x0_127}, to_apply=%region_4.3 | reduce-window | flops 8323072 | bytes 524292 | tf_op jit(solution)/shard_map/while/body/eval_jaxpr/cond/branch_1_fun/reduce_window_sum | solution.py:77
  235.5 3.4 %all-to-all-start.3 = ((bf16[2,128,256]{1,2,0:T(8,128)(2,1)}), bf16[2,128,256]{1,2,0:T(8,128)(2,1)S(1)}, u32[]{:S(2)}, u32[]{:S(2)}) async-start(bf16[2,128,256]{1,2,0:T(8,128)(2,1)} %bitcast.17), calls=%async_computation.3 | async-start | bytes 262144 | tf_op jit(solution)/shard_map/all_to_all | solution.py:211
  240.3 3.0 %all-to-all-done.3 = bf16[2,128,256]{1,2,0:T(8,128)(2,1)S(1)} async-done(((bf16[2,128,256]{1,2,0:T(8,128)(2,1)}), bf16[2,128,256]{1,2,0:T(8,128)(2,1)S(1)}, u32[]{:S(2)}, u32[]{:S(2)}) %all-to-all-start.3) | async-done | bytes 131104 | tf_op jit(solution)/shard_map/all_to_all | solution.py:211
  243.3 3.4 %all-to-all-start.7 = ((bf16[2,128,256]{1,2,0:T(8,128)(2,1)}), bf16[2,128,256]{1,2,0:T(8,128)(2,1)S(1)}, u32[]{:S(2)}, u32[]{:S(2)}) async-start(bf16[2,128,256]{1,2,0:T(8,128)(2,1)} %bitcast.38), calls=%async_computation.7 | async-start | bytes 262144 | tf_op jit(solution)/shard_map/all_to_all | solution.py:212
  246.8 2.1 fusion.69
  248.8 2.3 all-to-all-done.7
  251.1 2.9 %fusion.44 = bf16[128,2048]{1,0:T(8,128)(2,1)} fusion(f32[128,2048]{1,0:T(8,128)S(1)} %fusion.69, bf16[128,512]{0,1:T(8,128)(2,1)S(1)} %bitcast.150, bf16[512,2048]{1,0:T(8,128)(2,1)} %all-gather.9.cloned.1.call-done), kind=kOutput, calls=%fused_computation.60 | convolution fusion | flops 268959744 | bytes 3801088 | tf_op jit(solution)/shard_map/dot_general | solution.py:222
  254.0 25.0 %reduce-scatter.2.cloned.1.call-done = bf16[64,2048]{1,0:T(8,128)(2,1)} async-done(((bf16[128,2048]{1,0:T(8,128)(2,1)}), bf16[64,2048]{1,0:T(8,128)(2,1)}) %reduce-scatter.2.cloned.1.call-update) | async-done | bytes 262160 | tf_op jit(solution)/shard_map/reduce_scatter | solution.py:219
  (99 shorter events, 21.5 us)
Async XLA Ops:
  6.5 119.8 %copy-start = (f32[4,128]{1,0:T(4,128)S(1)}, f32[4,128]{1,0:T(4,128)}, u32[]{:S(2)}) copy-start(f32[4,128]{1,0:T(4,128)} %param.30) | copy-start | bytes 6148
  6.5 4.5 %copy-start.4 = (bf16[1024,512]{1,0:T(8,128)(2,1)S(1)}, bf16[1024,512]{1,0:T(8,128)(2,1)}, u32[]{:S(2)}) copy-start(bf16[1024,512]{1,0:T(8,128)(2,1)} %param.27) | copy-start | bytes 3145732
  6.5 132.5 %all-gather.11.cloned.1.call-start = ((), (), s32[]{:S(2)}) async-start(), calls=%async_computation.12 | async-start | bytes 1572864 | tf_op jit(solution)/shard_map/all_gather | solution.py:178
  11.1 5.5 %copy-start.5 = (bf16[1024,512]{1,0:T(8,128)(2,1)S(1)}, bf16[1024,512]{1,0:T(8,128)(2,1)}, u32[]{:S(2)}) copy-start(bf16[1024,512]{1,0:T(8,128)(2,1)} %param.26) | copy-start | bytes 3145732
  12.4 27.0 %all-to-all-start.4 = ((bf16[1024,2,256]{0,2,1:T(8,128)(2,1)}), bf16[1024,2,256]{0,2,1:T(8,128)(2,1)S(1)}, u32[]{:S(2)}, u32[]{:S(2)}) async-start(bf16[1024,2,256]{0,2,1:T(8,128)(2,1)} %bitcast.20), calls=%async_computation.4 | async-start | bytes 2097152 | tf_op jit(solution)/shard_map/all_to_all | solution.py:175
  17.9 25.9 %copy-start.6 = (bf16[1024,512]{1,0:T(8,128)(2,1)S(1)}, bf16[1024,512]{1,0:T(8,128)(2,1)}, u32[]{:S(2)}) copy-start(bf16[1024,512]{1,0:T(8,128)(2,1)} %param.28) | copy-start | bytes 3145732
  39.4 16.2 %all-to-all-start.6 = ((bf16[1024,2,256]{0,2,1:T(8,128)(2,1)}), bf16[1024,2,256]{0,2,1:T(8,128)(2,1)S(1)}, u32[]{:S(2)}, u32[]{:S(2)}) async-start(bf16[1024,2,256]{0,2,1:T(8,128)(2,1)} %bitcast.29), calls=%async_computation.6 | async-start | bytes 2097152 | tf_op jit(solution)/shard_map/all_to_all | solution.py:174
  43.0 203.7 %all-gather.7.cloned.1.call-start = ((), (), s32[]{:S(2)}) async-start(), calls=%async_computation.9 | async-start | bytes 3145728 | tf_op jit(solution)/shard_map/all_gather | solution.py:215
  55.6 28.7 %all-to-all-start.5 = ((bf16[1024,2,256]{0,2,1:T(8,128)(2,1)}), bf16[1024,2,256]{0,2,1:T(8,128)(2,1)S(1)}, u32[]{:S(2)}, u32[]{:S(2)}) async-start(bf16[1024,2,256]{0,2,1:T(8,128)(2,1)} %bitcast.144), calls=%async_computation.5 | async-start | bytes 2097152 | tf_op jit(solution)/shard_map/all_to_all | solution.py:176
  84.3 19.3 %all-to-all-start = ((bf16[1024,2,256]{0,2,1:T(8,128)(2,1)}), bf16[1024,2,256]{0,2,1:T(8,128)(2,1)}, u32[]{:S(2)}, u32[]{:S(2)}) async-start(bf16[1024,2,256]{0,2,1:T(8,128)(2,1)} %bitcast.145), calls=%async_computation | async-start | bytes 2097152 | tf_op jit(solution)/shard_map/all_to_all | solution.py:172
  103.7 17.4 %all-to-all-start.2 = ((bf16[1024,2,256]{0,2,1:T(8,128)(2,1)}), bf16[1024,2,256]{0,2,1:T(8,128)(2,1)}, u32[]{:S(2)}, u32[]{:S(2)}) async-start(bf16[1024,2,256]{0,2,1:T(8,128)(2,1)} %bitcast.146), calls=%async_computation.2 | async-start | bytes 2097152 | tf_op jit(solution)/shard_map/all_to_all | solution.py:173
  110.4 15.8 %copy-start.11 = (f32[4]{0:T(128)S(1)}, f32[4]{0:T(128)}, u32[]{:S(2)}) copy-start(f32[4]{0:T(128)} %param.29) | copy-start | bytes 52
  121.1 16.5 %all-to-all-start.1 = ((bf16[1024,2,256]{0,2,1:T(8,128)(2,1)}), bf16[1024,2,256]{0,2,1:T(8,128)(2,1)}, u32[]{:S(2)}, u32[]{:S(2)}) async-start(bf16[1024,2,256]{0,2,1:T(8,128)(2,1)} %bitcast.141), calls=%async_computation.1 | async-start | bytes 2097152 | tf_op jit(solution)/shard_map/all_to_all | solution.py:171
  125.5 125.7 %all-gather.9.cloned.1.call-start = ((), (), s32[]{:S(2)}) async-start(), calls=%async_computation.10 | async-start | bytes 3145728 | tf_op jit(solution)/shard_map/all_gather | solution.py:216
  132.6 6.5 %copy-start.7 = (bf16[2,1024,256]{2,1,0:T(8,128)(2,1)S(1)}, bf16[2,1024,256]{2,1,0:T(8,128)(2,1)}, u32[]{:S(2)}) copy-start(bf16[2,1024,256]{2,1,0:T(8,128)(2,1)} %copy.93) | copy-start | bytes 3145732
  139.1 6.2 %copy-start.1 = (bf16[1,256,2048]{2,1,0:T(8,128)(2,1)S(1)}, bf16[1,256,2048]{2,1,0:T(8,128)(2,1)}, u32[]{:S(2)}) copy-start(bf16[1,256,2048]{2,1,0:T(8,128)(2,1)} %all-gather.11.cloned.1.call-done) | copy-start | bytes 3145732
  143.4 7.8 %copy-start.3 = (bf16[2,1024,256]{2,1,0:T(8,128)(2,1)S(1)}, bf16[2,1024,256]{2,1,0:T(8,128)(2,1)}, u32[]{:S(2)}) copy-start(bf16[2,1024,256]{2,1,0:T(8,128)(2,1)} %copy.96) | copy-start | bytes 3145732
  182.0 29.5 %copy-start.2 = (bf16[2,1024,256]{2,1,0:T(8,128)(2,1)S(1)}, bf16[2,1024,256]{2,1,0:T(8,128)(2,1)}, u32[]{:S(2)}) copy-start(bf16[2,1024,256]{2,1,0:T(8,128)(2,1)} %copy.88) | copy-start | bytes 3145732
  234.7 4.2 %copy-start.8 = (f32[2,128,2,128]{1,3,2,0:T(8,128)S(1)}, f32[2,128,2,128]{1,3,2,0:T(8,128)}, u32[]{:S(2)}) copy-start(f32[2,128,2,128]{1,3,2,0:T(8,128)} %copy.104) | copy-start | bytes 786436
  234.7 4.2 %copy-start.9 = (f32[2,128,2,128]{3,2,1,0:T(2,128)S(1)}, f32[2,128,2,128]{3,2,1,0:T(2,128)}, u32[]{:S(2)}) copy-start(f32[2,128,2,128]{3,2,1,0:T(2,128)} %get-tuple-element.520) | copy-start | bytes 786436
  235.5 7.8 %all-to-all-start.3 = ((bf16[2,128,256]{1,2,0:T(8,128)(2,1)}), bf16[2,128,256]{1,2,0:T(8,128)(2,1)S(1)}, u32[]{:S(2)}, u32[]{:S(2)}) async-start(bf16[2,128,256]{1,2,0:T(8,128)(2,1)} %bitcast.17), calls=%async_computation.3 | async-start | bytes 262144 | tf_op jit(solution)/shard_map/all_to_all | solution.py:211
  238.9 0.7 copy-start.10
  243.3 7.8 %all-to-all-start.7 = ((bf16[2,128,256]{1,2,0:T(8,128)(2,1)}), bf16[2,128,256]{1,2,0:T(8,128)(2,1)S(1)}, u32[]{:S(2)}, u32[]{:S(2)}) async-start(bf16[2,128,256]{1,2,0:T(8,128)(2,1)} %bitcast.38), calls=%async_computation.7 | async-start | bytes 262144 | tf_op jit(solution)/shard_map/all_to_all | solution.py:212
  246.7 32.4 %reduce-scatter.2.cloned.1.call-start = ((), (), s32[]{:S(2)}) async-start(), calls=%async_computation.11 | async-start | bytes 786432 | tf_op jit(solution)/shard_map/reduce_scatter | solution.py:219
Sparse Core Ops, SparseCore 0:
  11.2 31.5 all-gather.10
  45.4 49.9 all-gather.6
  127.8 34.1 all-gather.8
  254.2 24.8 reduce-scatter.1
where the time goes:
time: 287 us; the launch traced here: 286 us
  waiting for transfers between devices  112 us (39%)
  blocking collectives  60.2 us (21%)
  local copies, waits for them, and re-layouts  35.2 us (12%)
  starting transfers between devices  31.5 us (11%)
  matrix products  20.6 us (7%)
  between operations  13.5 us (5%)
  other arithmetic  11.9 us (4%)
    all_gather x2, blocking collectives, carried_in(): lax.all_gather(a.astype(kind), axis)  26.1 us
    reduce_scatter x1, waiting for transfers between devices, body(): lax.psum_scatter((jnp.dot(attn_flat, full_attn, preferred_element_type=jn...  25 us
    all_to_all x1, waiting for transfers between devices, body(): lax.all_to_all(weights[5], 'fs', split_axis=1, concat_axis=0, tiled=True)  22.8 us
    all_to_all x1, waiting for transfers between devices, body(): lax.all_to_all(weights[4], 'fs', split_axis=1, concat_axis=0, tiled=True)  21.6 us
    all_gather x1, blocking collectives, stick_mixer(): key_all = lax.all_gather(key_rows, 'sp', axis=1, tiled=True)  16.5 us
    all_gather x1, blocking collectives, stick_mixer(): value_all = lax.all_gather(value_rows, 'sp', axis=1, tiled=True)  14.9 us
    all_to_all x1, waiting for transfers between devices, body(): lax.all_to_all(weights[1], 'fs', split_axis=1, concat_axis=0, tiled=True)  12.6 us
    unnamed x31, local copies, waits for them, and re-layouts  10.9 us
  transfers between devices with their start and end apart: 12, of which 9 were waited for; matrix products, arithmetic and copies ran while one was open for 22% of the time, Pallas kernels for 0%

commit v1 on v0

--- a/solution.py
+++ b/solution.py
@@ -169,7 +169,12 @@
     weights = (attn_query, attn_key, attn_value, rec_query, rec_forget, rec_input)
     turned = (
         lax.all_to_all(weights[0], "fs", split_axis=1, concat_axis=0, tiled=True),
-        lax.all_to_all(weights[1], "fs", split_axis=1, concat_axis=0, tiled=True),
+        jnp.concatenate(
+            lax.all_to_all(
+                jnp.stack(jnp.split(weights[1], lax.axis_size("fs"), axis=1)), "fs", 0, 0
+            ),
+            axis=0,
+        ),
         lax.all_to_all(weights[2], "fs", split_axis=1, concat_axis=0, tiled=True),
         lax.all_to_all(weights[3], "fs", split_axis=1, concat_axis=0, tiled=True),
         lax.all_to_all(weights[4], "fs", split_axis=1, concat_axis=0, tiled=True),

time: 287 us -> 273 us (0.951)
  waiting for transfers between devices: 112 us -> 101 us
  local copies, waits for them, and re-layouts: 35.2 us -> 29.3 us
    all_to_all x1, waiting for transfers between devices: 12.6 us -> 0.01 us  [body(): lax.all_to_all(jnp.stack(jnp.split(weights[1], lax.axis_size('fs'), axis=...]
    unnamed x31 -> x32, local copies, waits for them, and re-layouts: 10.9 us -> 8.56 us
  transfers between devices with their start and end apart: 12 -> 12, of which waited for: 9 -> 8; matrix products, arithmetic and copies ran while one was open for 22% -> 21% of each run, Pallas kernels for 0% -> 0%
where the time goes in v1:
time: 273 us; the launch traced here: 271 us
  waiting for transfers between devices  101 us (37%)
  blocking collectives  61.3 us (22%)
  starting transfers between devices  32.6 us (12%)
  local copies, waits for them, and re-layouts  29.3 us (11%)
  matrix products  21.5 us (8%)
  between operations  13.5 us (5%)
  other arithmetic  12 us (4%)
    reduce_scatter x1, waiting for transfers between devices, body(): lax.psum_scatter((jnp.dot(attn_flat, full_attn, preferred_element_type=jn...  27.2 us
    all_gather x2, blocking collectives, carried_in(): lax.all_gather(a.astype(kind), axis)  26.7 us
    all_to_all x1, waiting for transfers between devices, body(): lax.all_to_all(weights[5], 'fs', split_axis=1, concat_axis=0, tiled=True)  22.7 us
    all_to_all x1, waiting for transfers between devices, body(): lax.all_to_all(weights[4], 'fs', split_axis=1, concat_axis=0, tiled=True)  20.9 us
    all_gather x1, blocking collectives, stick_mixer(): key_all = lax.all_gather(key_rows, 'sp', axis=1, tiled=True)  16.4 us
    all_gather x1, blocking collectives, stick_mixer(): value_all = lax.all_gather(value_rows, 'sp', axis=1, tiled=True)  15.6 us
    all_to_all x1, waiting for transfers between devices, body(): lax.all_to_all(weights[3], 'fs', split_axis=1, concat_axis=0, tiled=True)  12 us
    all_to_all x1, waiting for transfers between devices, body(): lax.all_to_all(weights[2], 'fs', split_axis=1, concat_axis=0, tiled=True)  9.1 us
  transfers between devices with their start and end apart: 12, of which 8 were waited for; matrix products, arithmetic and copies ran while one was open for 21% of the time, Pallas kernels for 0%

profile of v1, /device:TPU:0, one launch (start us, length us, event | category | flops | bytes accessed | tf_op | source)
XLA Modules:
  0.0 271.2 jit_solution(16683148303905917829)
XLA Ops:
  6.5 2.6 all_gather.28
  9.4 1.7 fusion.54
  11.1 1.3 copy.86
  12.5 4.2 %all-to-all-start.4 = ((bf16[1024,2,256]{0,2,1:T(8,128)(2,1)}), bf16[1024,2,256]{0,2,1:T(8,128)(2,1)S(1)}, u32[]{:S(2)}, u32[]{:S(2)}) async-start(bf16[1024,2,256]{0,2,1:T(8,128)(2,1)} %bitcast.20), calls=%async_computation.4 | async-start | bytes 2097152 | tf_op jit(solution)/shard_map/all_to_all | solution.py:180
  17.5 1.3 copy.92
  18.8 20.9 %all-to-all-done.4 = bf16[1024,2,256]{0,2,1:T(8,128)(2,1)S(1)} async-done(((bf16[1024,2,256]{0,2,1:T(8,128)(2,1)}), bf16[1024,2,256]{0,2,1:T(8,128)(2,1)S(1)}, u32[]{:S(2)}, u32[]{:S(2)}) %all-to-all-start.4) | async-done | bytes 1048608 | tf_op jit(solution)/shard_map/all_to_all | solution.py:180
  39.7 3.6 %all-to-all-start.6 = ((bf16[1024,2,256]{0,2,1:T(8,128)(2,1)}), bf16[1024,2,256]{0,2,1:T(8,128)(2,1)S(1)}, u32[]{:S(2)}, u32[]{:S(2)}) async-start(bf16[1024,2,256]{0,2,1:T(8,128)(2,1)} %bitcast.29), calls=%async_computation.6 | async-start | bytes 2097152 | tf_op jit(solution)/shard_map/all_to_all | solution.py:179
  43.3 1.3 copy.89
  44.6 12.0 %all-to-all-done.6 = bf16[1024,2,256]{0,2,1:T(8,128)(2,1)S(1)} async-done(((bf16[1024,2,256]{0,2,1:T(8,128)(2,1)}), bf16[1024,2,256]{0,2,1:T(8,128)(2,1)S(1)}, u32[]{:S(2)}, u32[]{:S(2)}) %all-to-all-start.6) | async-done | bytes 1048608 | tf_op jit(solution)/shard_map/all_to_all | solution.py:179
  56.6 3.6 %all-to-all-start.5 = ((bf16[1024,2,256]{0,2,1:T(8,128)(2,1)}), bf16[1024,2,256]{0,2,1:T(8,128)(2,1)S(1)}, u32[]{:S(2)}, u32[]{:S(2)}) async-start(bf16[1024,2,256]{0,2,1:T(8,128)(2,1)} %bitcast.145), calls=%async_computation.5 | async-start | bytes 2097152 | tf_op jit(solution)/shard_map/all_to_all | solution.py:181
  60.2 2.3 copy.81
  62.5 22.7 %all-to-all-done.5 = bf16[1024,2,256]{0,2,1:T(8,128)(2,1)S(1)} async-done(((bf16[1024,2,256]{0,2,1:T(8,128)(2,1)}), bf16[1024,2,256]{0,2,1:T(8,128)(2,1)S(1)}, u32[]{:S(2)}, u32[]{:S(2)}) %all-to-all-start.5) | async-done | bytes 1048608 | tf_op jit(solution)/shard_map/all_to_all | solution.py:181
  85.1 4.4 %all-to-all-start.2 = ((bf16[1024,2,256]{0,2,1:T(8,128)(2,1)}), bf16[1024,2,256]{0,2,1:T(8,128)(2,1)}, u32[]{:S(2)}, u32[]{:S(2)}) async-start(bf16[1024,2,256]{0,2,1:T(8,128)(2,1)} %bitcast.146), calls=%async_computation.2 | async-start | bytes 2097152 | tf_op jit(solution)/shard_map/all_to_all | solution.py:178
  89.5 2.3 copy.79
  91.8 9.1 %all-to-all-done.2 = bf16[1024,2,256]{0,2,1:T(8,128)(2,1)} async-done(((bf16[1024,2,256]{0,2,1:T(8,128)(2,1)}), bf16[1024,2,256]{0,2,1:T(8,128)(2,1)}, u32[]{:S(2)}, u32[]{:S(2)}) %all-to-all-start.2) | async-done | bytes 1048608 | tf_op jit(solution)/shard_map/all_to_all | solution.py:178
  100.9 4.5 %all-to-all-start.1 = ((bf16[1024,2,256]{0,2,1:T(8,128)(2,1)}), bf16[1024,2,256]{0,2,1:T(8,128)(2,1)}, u32[]{:S(2)}, u32[]{:S(2)}) async-start(bf16[1024,2,256]{0,2,1:T(8,128)(2,1)} %bitcast.142), calls=%async_computation.1 | async-start | bytes 2097152 | tf_op jit(solution)/shard_map/all_to_all | solution.py:171
  106.3 1.3 slice_bitcast_fusion.1
  108.6 1.3 copy.87
  110.0 1.3 copy.93
  111.3 1.3 copy.90
  112.6 1.5 copy.82
  114.1 1.8 all-to-all-done.1
  115.9 4.4 %all-to-all-start = ((bf16[2,1024,256]{2,1,0:T(8,128)(2,1)}), bf16[2,1024,256]{2,1,0:T(8,128)(2,1)}, u32[]{:S(2)}, u32[]{:S(2)}) async-start(bf16[2,1024,256]{2,1,0:T(8,128)(2,1)} %pad_maximum_fusion), calls=%async_computation | async-start | bytes 2097152 | tf_op jit(solution)/shard_map/all_to_all | solution.py:173
  120.4 2.3 copy.80
  122.6 2.5 fusion.51
  125.1 1.9 div.26
  127.0 2.4 fusion.46
  129.4 1.8 reshape.148
  133.4 1.8 fusion.66
  136.2 6.9 %while.43 = (s32[]{:T(128)}, f32[2,2,128,128]{3,2,1,0:T(8,128)S(1)}, f32[2,2,2,64,128]{4,3,0,2,1:T(8,128)}, f32[2,2,2,64,128]{4,3,2,1,0:T(8,128)}, f32[2,2,2,64,...) while((s32[]{:T(128)}, ...), condition=%wide.region_11.12_spmd.clone, body=%wide.region_9.11_spmd.clone.sunk | while | flops 153571328 | bytes 3239036 | solution.py:125
  145.3 1.3 exponential_multiply_fusion
  147.5 11.0 %all-gather.1 = bf16[8,1,2,128]{3,2,1,0:T(2,128)(2,1)S(1)} all-gather(bf16[2,1,2,128]{3,2,1,0:T(2,128)(2,1)S(1)} %slice.12), channel_id=3, replica_groups=mesh['grp'=2,'sp'=4,'fs'=2,'tp'=2] {'sp'}, dimensions={0}, use_global_device_ids=true | all-gather | bytes 5120 | tf_op jit(solution)/shard_map/all_gather | solution.py:18
  158.5 15.7 %all-gather.2 = bf16[8,2,128,128]{3,2,1,0:T(8,128)(2,1)} all-gather(bf16[2,2,128,128]{3,2,1,0:T(8,128)(2,1)S(1)} %convert_element_type.118), channel_id=4, replica_groups=mesh['grp'=2,'sp'=4,'fs'=2,'tp'=2] {'sp'}, dimensions={0}, use_global_device_ids=true | all-gather | bytes 655360 | tf_op jit(solution)/shard_map/all_gather | solution.py:18
  174.2 1.7 convolution_convert_fusion.5
  175.9 16.4 %all_gather.30 = bf16[2,512,2,128]{3,1,2,0:T(8,128)(2,1)} all-gather(bf16[2,128,2,128]{3,1,2,0:T(8,128)(2,1)S(1)} %copy.78), channel_id=1, replica_groups=mesh['grp'=2,'sp'=4,'fs'=2,'tp'=2] {'sp'}, dimensions={1}, use_global_device_ids=true | all-gather | bytes 655360 | tf_op jit(solution)/shard_map/all_gather | solution.py:92
  192.8 15.6 %all_gather.31 = bf16[2,512,2,128]{3,1,2,0:T(8,128)(2,1)} all-gather(bf16[2,128,2,128]{3,1,2,0:T(8,128)(2,1)S(1)} %copy.83), channel_id=1, replica_groups=mesh['grp'=2,'sp'=4,'fs'=2,'tp'=2] {'sp'}, dimensions={1}, use_global_device_ids=true | all-gather | bytes 655360 | tf_op jit(solution)/shard_map/all_gather | solution.py:93
  209.0 7.5 %while.42 = (s32[]{:T(128)}, f32[4,2,128,2,128]{4,2,3,1,0:T(8,128)S(1)}, f32[4,2,128,2]{2,3,1,0:T(2,128)S(1)}, s32[]{:T(128)}, bf16[2,512,2,128]{3,1,2,0:T(8,128...) while((s32[]{:T(128)}, ...), condition=%wide.region_6.7_spmd.clone, body=%wide.region_1.6_spmd.clone.sunk | while | flops 43925260 | bytes 2286935 | solution.py:101
  209.1 7.3 %conditional.3 = ((f32[4,2,128,2,128]{4,2,3,1,0:T(8,128)S(1)}, f32[4,2,128,2]{2,3,1,0:T(2,128)S(1)})) conditional(s32[]{:T(128)} %convert_element_type.168, (f32[4,2,128,2,128]{4,2,3,1,0:T(8,128)S(1)}, f32[4,2,128,2]{2,3,1,0:T(2,128)S(1)}) %tuple.101, (s32[]{:T(128)}, s32[]{:T(128)}, bf16[2,512,2,128]{3,1,2,0:T(8,128)(2,1)}, ...), branch_computations={%region_2.0_spmd, %region_3.5_spmd} | conditional | flops 43925256 | bytes 2286220 | solution.py:90
  209.2 1.3 fusion.20
  210.5 4.4 %reduce_window_sum.43 = f32[2,2,128,128]{2,3,1,0:T(8,128)S(1)} reduce-window(f32[2,2,128,128]{2,3,1,0:T(8,128)S(1)} %get-tuple-element.514, f32[]{:T(128)} %constant.131.clone), window={size=1x1x1x128 pad=0_0x0_0x0_0x0_127}, to_apply=%region_4.3 | reduce-window | flops 8323072 | bytes 524292 | tf_op jit(solution)/shard_map/while/body/eval_jaxpr/cond/branch_1_fun/reduce_window_sum | solution.py:77
  214.9 1.5 fusion.4
  217.8 4.4 %all-to-all-start.3 = ((bf16[2,128,256]{1,2,0:T(8,128)(2,1)}), bf16[2,128,256]{1,2,0:T(8,128)(2,1)S(1)}, u32[]{:S(2)}, u32[]{:S(2)}) async-start(bf16[2,128,256]{1,2,0:T(8,128)(2,1)} %bitcast.17), calls=%async_computation.3 | async-start | bytes 262144 | tf_op jit(solution)/shard_map/all_to_all | solution.py:216
  223.6 3.1 %all-to-all-done.3 = bf16[2,128,256]{1,2,0:T(8,128)(2,1)S(1)} async-done(((bf16[2,128,256]{1,2,0:T(8,128)(2,1)}), bf16[2,128,256]{1,2,0:T(8,128)(2,1)S(1)}, u32[]{:S(2)}, u32[]{:S(2)}) %all-to-all-start.3) | async-done | bytes 131104 | tf_op jit(solution)/shard_map/all_to_all | solution.py:216
  226.7 3.4 %all-to-all-start.7 = ((bf16[2,128,256]{1,2,0:T(8,128)(2,1)}), bf16[2,128,256]{1,2,0:T(8,128)(2,1)S(1)}, u32[]{:S(2)}, u32[]{:S(2)}) async-start(bf16[2,128,256]{1,2,0:T(8,128)(2,1)} %bitcast.38), calls=%async_computation.7 | async-start | bytes 262144 | tf_op jit(solution)/shard_map/all_to_all | solution.py:217
  230.2 2.1 fusion.69
  232.2 2.3 all-to-all-done.7
  234.6 2.9 %fusion.44 = bf16[128,2048]{1,0:T(8,128)(2,1)} fusion(f32[128,2048]{1,0:T(8,128)S(1)} %fusion.69, bf16[128,512]{0,1:T(8,128)(2,1)S(1)} %bitcast.150, bf16[512,2048]{1,0:T(8,128)(2,1)} %all-gather.9.cloned.1.call-done), kind=kOutput, calls=%fused_computation.60 | convolution fusion | flops 268959744 | bytes 3801088 | tf_op jit(solution)/shard_map/dot_general | solution.py:227
  237.5 27.2 %reduce-scatter.2.cloned.1.call-done = bf16[64,2048]{1,0:T(8,128)(2,1)} async-done(((bf16[128,2048]{1,0:T(8,128)(2,1)}), bf16[64,2048]{1,0:T(8,128)(2,1)}) %reduce-scatter.2.cloned.1.call-update) | async-done | bytes 262160 | tf_op jit(solution)/shard_map/reduce_scatter | solution.py:224
  (101 shorter events, 19.9 us)
Async XLA Ops:
  6.5 99.7 %copy-start = (f32[4,128]{1,0:T(4,128)S(1)}, f32[4,128]{1,0:T(4,128)}, u32[]{:S(2)}) copy-start(f32[4,128]{1,0:T(4,128)} %param.30) | copy-start | bytes 6148
  6.5 4.6 %copy-start.4 = (bf16[1024,512]{1,0:T(8,128)(2,1)S(1)}, bf16[1024,512]{1,0:T(8,128)(2,1)}, u32[]{:S(2)}) copy-start(bf16[1024,512]{1,0:T(8,128)(2,1)} %param.27) | copy-start | bytes 3145732
  6.5 116.1 %all-gather.11.cloned.1.call-start = ((), (), s32[]{:S(2)}) async-start(), calls=%async_computation.12 | async-start | bytes 1572864 | tf_op jit(solution)/shard_map/all_gather | solution.py:183
  12.5 5.0 %copy-start.5 = (bf16[1024,512]{1,0:T(8,128)(2,1)S(1)}, bf16[1024,512]{1,0:T(8,128)(2,1)}, u32[]{:S(2)}) copy-start(bf16[1024,512]{1,0:T(8,128)(2,1)} %param.26) | copy-start | bytes 3145732
  12.5 27.2 %all-to-all-start.4 = ((bf16[1024,2,256]{0,2,1:T(8,128)(2,1)}), bf16[1024,2,256]{0,2,1:T(8,128)(2,1)S(1)}, u32[]{:S(2)}, u32[]{:S(2)}) async-start(bf16[1024,2,256]{0,2,1:T(8,128)(2,1)} %bitcast.20), calls=%async_computation.4 | async-start | bytes 2097152 | tf_op jit(solution)/shard_map/all_to_all | solution.py:180
  16.7 213.5 %all-gather.7.cloned.1.call-start = ((), (), s32[]{:S(2)}) async-start(), calls=%async_computation.9 | async-start | bytes 3145728 | tf_op jit(solution)/shard_map/all_gather | solution.py:220
  17.4 25.8 %copy-start.6 = (bf16[1024,512]{1,0:T(8,128)(2,1)S(1)}, bf16[1024,512]{1,0:T(8,128)(2,1)}, u32[]{:S(2)}) copy-start(bf16[1024,512]{1,0:T(8,128)(2,1)} %param.28) | copy-start | bytes 3145732
  39.7 16.9 %all-to-all-start.6 = ((bf16[1024,2,256]{0,2,1:T(8,128)(2,1)}), bf16[1024,2,256]{0,2,1:T(8,128)(2,1)S(1)}, u32[]{:S(2)}, u32[]{:S(2)}) async-start(bf16[1024,2,256]{0,2,1:T(8,128)(2,1)} %bitcast.29), calls=%async_computation.6 | async-start | bytes 2097152 | tf_op jit(solution)/shard_map/all_to_all | solution.py:179
  56.6 28.5 %all-to-all-start.5 = ((bf16[1024,2,256]{0,2,1:T(8,128)(2,1)}), bf16[1024,2,256]{0,2,1:T(8,128)(2,1)S(1)}, u32[]{:S(2)}, u32[]{:S(2)}) async-start(bf16[1024,2,256]{0,2,1:T(8,128)(2,1)} %bitcast.145), calls=%async_computation.5 | async-start | bytes 2097152 | tf_op jit(solution)/shard_map/all_to_all | solution.py:181
  85.1 15.8 %all-to-all-start.2 = ((bf16[1024,2,256]{0,2,1:T(8,128)(2,1)}), bf16[1024,2,256]{0,2,1:T(8,128)(2,1)}, u32[]{:S(2)}, u32[]{:S(2)}) async-start(bf16[1024,2,256]{0,2,1:T(8,128)(2,1)} %bitcast.146), calls=%async_computation.2 | async-start | bytes 2097152 | tf_op jit(solution)/shard_map/all_to_all | solution.py:178
  91.8 14.4 %copy-start.12 = (f32[4]{0:T(128)S(1)}, f32[4]{0:T(128)}, u32[]{:S(2)}) copy-start(f32[4]{0:T(128)} %param.29) | copy-start | bytes 52
  100.9 15.0 %all-to-all-start.1 = ((bf16[1024,2,256]{0,2,1:T(8,128)(2,1)}), bf16[1024,2,256]{0,2,1:T(8,128)(2,1)}, u32[]{:S(2)}, u32[]{:S(2)}) async-start(bf16[1024,2,256]{0,2,1:T(8,128)(2,1)} %bitcast.142), calls=%async_computation.1 | async-start | bytes 2097152 | tf_op jit(solution)/shard_map/all_to_all | solution.py:171
  105.4 129.2 %all-gather.9.cloned.1.call-start = ((), (), s32[]{:S(2)}) async-start(), calls=%async_computation.10 | async-start | bytes 3145728 | tf_op jit(solution)/shard_map/all_gather | solution.py:221
  114.1 8.6 %copy-start.7 = (bf16[2,1024,256]{2,1,0:T(8,128)(2,1)S(1)}, bf16[2,1024,256]{2,1,0:T(8,128)(2,1)}, u32[]{:S(2)}) copy-start(bf16[2,1024,256]{2,1,0:T(8,128)(2,1)} %copy.87) | copy-start | bytes 3145732
  115.9 58.2 %all-to-all-start = ((bf16[2,1024,256]{2,1,0:T(8,128)(2,1)}), bf16[2,1024,256]{2,1,0:T(8,128)(2,1)}, u32[]{:S(2)}, u32[]{:S(2)}) async-start(bf16[2,1024,256]{2,1,0:T(8,128)(2,1)} %pad_maximum_fusion), calls=%async_computation | async-start | bytes 2097152 | tf_op jit(solution)/shard_map/all_to_all | solution.py:173
  122.6 4.4 %copy-start.1 = (bf16[1,256,2048]{2,1,0:T(8,128)(2,1)S(1)}, bf16[1,256,2048]{2,1,0:T(8,128)(2,1)}, u32[]{:S(2)}) copy-start(bf16[1,256,2048]{2,1,0:T(8,128)(2,1)} %all-gather.11.cloned.1.call-done) | copy-start | bytes 3145732
  125.1 6.1 %copy-start.3 = (bf16[2,1024,256]{2,1,0:T(8,128)(2,1)S(1)}, bf16[2,1024,256]{2,1,0:T(8,128)(2,1)}, u32[]{:S(2)}) copy-start(bf16[2,1024,256]{2,1,0:T(8,128)(2,1)} %copy.90) | copy-start | bytes 3145732
  143.1 3.6 %copy-start.10 = (f32[2,2,2,64,128]{4,3,0,2,1:T(8,128)S(1)}, f32[2,2,2,64,128]{4,3,0,2,1:T(8,128)}, u32[]{:S(2)}) copy-start(f32[2,2,2,64,128]{4,3,0,2,1:T(8,128)} %get-tuple-element.373) | copy-start | bytes 786436
  175.9 32.5 %copy-start.2 = (bf16[2,1024,256]{2,1,0:T(8,128)(2,1)S(1)}, bf16[2,1024,256]{2,1,0:T(8,128)(2,1)}, u32[]{:S(2)}) copy-start(bf16[2,1024,256]{2,1,0:T(8,128)(2,1)} %copy.80) | copy-start | bytes 3145732
  217.0 5.2 %copy-start.8 = (f32[2,128,2,128]{1,3,2,0:T(8,128)S(1)}, f32[2,128,2,128]{1,3,2,0:T(8,128)}, u32[]{:S(2)}) copy-start(f32[2,128,2,128]{1,3,2,0:T(8,128)} %copy.98) | copy-start | bytes 786436
  217.0 5.2 %copy-start.9 = (f32[2,128,2,128]{3,2,1,0:T(2,128)S(1)}, f32[2,128,2,128]{3,2,1,0:T(2,128)}, u32[]{:S(2)}) copy-start(f32[2,128,2,128]{3,2,1,0:T(2,128)} %get-tuple-element.522) | copy-start | bytes 786436
  217.8 8.9 %all-to-all-start.3 = ((bf16[2,128,256]{1,2,0:T(8,128)(2,1)}), bf16[2,128,256]{1,2,0:T(8,128)(2,1)S(1)}, u32[]{:S(2)}, u32[]{:S(2)}) async-start(bf16[2,128,256]{1,2,0:T(8,128)(2,1)} %bitcast.17), calls=%async_computation.3 | async-start | bytes 262144 | tf_op jit(solution)/shard_map/all_to_all | solution.py:216
  222.2 0.7 copy-start.11
  226.7 7.8 %all-to-all-start.7 = ((bf16[2,128,256]{1,2,0:T(8,128)(2,1)}), bf16[2,128,256]{1,2,0:T(8,128)(2,1)S(1)}, u32[]{:S(2)}, u32[]{:S(2)}) async-start(bf16[2,128,256]{1,2,0:T(8,128)(2,1)} %bitcast.38), calls=%async_computation.7 | async-start | bytes 262144 | tf_op jit(solution)/shard_map/all_to_all | solution.py:217
  230.1 34.5 %reduce-scatter.2.cloned.1.call-start = ((), (), s32[]{:S(2)}) async-start(), calls=%async_computation.11 | async-start | bytes 786432 | tf_op jit(solution)/shard_map/reduce_scatter | solution.py:224
Sparse Core Ops, SparseCore 0:
  11.3 31.6 all-gather.10
  44.5 45.7 all-gather.6
  107.8 44.8 all-gather.8
  237.6 27.0 reduce-scatter.1
